TPU v7x, 32 devices: a whole 2x2x4 slice. The times are simulated.
32 devices in a mesh: fs: 8 (over z, y), tp: 4 (over x, core).
Axes of the slice: x: 2, y: 2, z: 4, core: 2. Of those that a mesh axis runs over, the one named last changes fastest.
Arguments:
- tokens: bfloat16 [4096, 2048], P('fs', 'tp'), may hold values from -6 to 6
- mixer_gain: float32 [2048], replicated, may hold values from 0.1 to 1.9
- recur_in: bfloat16 [2048, 1024], P('fs', 'tp'), may hold values from -0.125 to 0.125
- branch_in: bfloat16 [2048, 1024], P('fs', 'tp'), may hold values from -0.125 to 0.125
- conv_taps: bfloat16 [4, 1024], replicated, may hold values from -3 to 3
- recur_gate: bfloat16 [2, 16, 64, 64], replicated, may hold values from -0.75 to 0.75
- input_gate: bfloat16 [2, 16, 64, 64], replicated, may hold values from -0.75 to 0.75
- decay_param: float32 [2, 1024], replicated, may hold values from 3.5 to 11
- recur_gain: float32 [1024], replicated, may hold values from 0.1 to 1.9
- recur_out: bfloat16 [1024, 2048], P('tp', 'fs'), may hold values from -0.1875 to 0.1875
- mixer_post: float32 [2048], replicated, may hold values from 0.1 to 1.9
- channel_gain: float32 [2048], replicated, may hold values from 0.1 to 1.9
- hidden_gate: bfloat16 [2048, 5632], P('fs', 'tp'), may hold values from -0.125 to 0.125
- hidden_up: bfloat16 [2048, 5632], P('fs', 'tp'), may hold values from -0.125 to 0.125
- hidden_down: bfloat16 [5632, 2048], P('tp', 'fs'), may hold values from -0.078125 to 0.078125
- channel_post: float32 [2048], replicated, may hold values from 0.1 to 1.9
Outputs:
- layer_out: bfloat16 [4096, 2048], P('fs', 'tp')
All inputs are finite; a program needn't handle non-finite values.
Results may differ from a plain program's by a relative error of at most 0.018.
Values may be sent and summed in bfloat16 or wider, within the bound.
A program may use at most 64 MiB of HBM per device.

v0:
```python
import jax
import jax.numpy as jnp
from jax import lax
from jax.sharding import PartitionSpec as P

D = 2048
BLOCK = 64
EPS = 1e-06
SHRINK = 8.0


def rms_scale(values, gain):
    return values * lax.rsqrt(jnp.mean(values * values, axis=-1, keepdims=True) + EPS) * gain


def linear_scan(decay, inflow, reverse):

    def combine(former, latter):
        return (former[0] * latter[0], latter[0] * former[1] + latter[1])

    return lax.associative_scan(combine, (decay, inflow), axis=0, reverse=reverse)[1]


def short_conv(recur_x, taps):
    length = recur_x.shape[0]
    padded = jnp.pad(recur_x.astype(jnp.float32), ((2, 1), (0, 0)))
    total = taps[0] * padded[0:length]
    for position in range(1, taps.shape[0]):
        total = total + taps[position] * padded[position : position + length]
    return total


def recurrence(conv_out, rate_weight, inlet_weight, decay_row, reverse):
    length, width = conv_out.shape
    grouped = conv_out.reshape(length, rate_weight.shape[0], rate_weight.shape[1])
    rate = jax.nn.sigmoid(
        jnp.einsum(
            "lhi,hij->lhj",
            grouped,
            rate_weight.astype(jnp.float32),
            precision=lax.Precision.HIGHEST,
        ).reshape(length, width)
    )
    inlet = jax.nn.sigmoid(
        jnp.einsum(
            "lhi,hij->lhj",
            grouped,
            inlet_weight.astype(jnp.float32),
            precision=lax.Precision.HIGHEST,
        ).reshape(length, width)
    )
    log_decay = -SHRINK * rate * jax.nn.softplus(-decay_row)
    inflow = conv_out * inlet * jnp.sqrt(-jnp.expm1(2.0 * log_decay))
    return linear_scan(jnp.exp(log_decay), inflow, reverse)


def add_slab(source, piece):
    return jnp.dot(source, piece, preferred_element_type=jnp.float32)


def on_device(
    tokens,
    mixer_gain,
    recur_in,
    branch_in,
    conv_taps,
    recur_gate,
    input_gate,
    decay_param,
    recur_gain,
    recur_out,
    mixer_post,
    channel_gain,
    hidden_gate,
    hidden_up,
    hidden_down,
    channel_post,
):
    rank_tp = lax.axis_index("tp")
    feature_width = tokens.shape[1]
    channel_width = recur_in.shape[1]
    group_count = channel_width // BLOCK
    feature_start = rank_tp * feature_width
    channel_start = rank_tp * channel_width
    gathered_in = lax.all_gather(tokens, "tp", axis=1, tiled=True)
    gathered_float = gathered_in.astype(jnp.float32)
    normed_in = rms_scale(gathered_float, mixer_gain).astype(jnp.bfloat16)

    def add_mixer(piece):
        return add_slab(normed_in, piece)

    recur_total = add_mixer(lax.all_gather(recur_in, "fs", axis=0, tiled=True))
    branch_total = add_mixer(lax.all_gather(branch_in, "fs", axis=0, tiled=True))
    recur_x = recur_total.astype(jnp.bfloat16)
    branch_x = branch_total.astype(jnp.bfloat16)
    taps = lax.dynamic_slice_in_dim(conv_taps, channel_start, channel_width, 1).astype(jnp.float32)
    conv_out = short_conv(recur_x, taps)
    group_start = rank_tp * group_count
    rate_own = lax.dynamic_slice_in_dim(recur_gate, group_start, group_count, 1)
    inlet_own = lax.dynamic_slice_in_dim(input_gate, group_start, group_count, 1)
    decay_own = lax.dynamic_slice_in_dim(decay_param, channel_start, channel_width, 1)
    forward = recurrence(conv_out, rate_own[0], inlet_own[0], decay_own[0], False)
    backward = recurrence(conv_out, rate_own[1], inlet_own[1], decay_own[1], True)
    mixed = (forward + backward) * jax.nn.gelu(branch_x.astype(jnp.float32))
    gain_own = lax.dynamic_slice_in_dim(recur_gain, channel_start, channel_width, 0)
    recur_y = (mixed * gain_own).astype(jnp.bfloat16)
    branch_part = jnp.dot(
        recur_y,
        lax.all_gather(recur_out, "fs", axis=1, tiled=True),
        preferred_element_type=jnp.float32,
    )
    branch_sum = lax.psum(branch_part.astype(jnp.bfloat16), "tp").astype(jnp.float32)
    mid_full = (gathered_float + rms_scale(branch_sum, mixer_post)).astype(jnp.bfloat16)
    mid_own = lax.dynamic_slice_in_dim(mid_full, feature_start, feature_width, 1)
    channel_in = rms_scale(mid_full.astype(jnp.float32), channel_gain).astype(jnp.bfloat16)

    def add_channel(piece):
        return add_slab(channel_in, piece)

    gate_total = add_channel(lax.all_gather(hidden_gate, "fs", axis=0, tiled=True))
    up_total = add_channel(lax.all_gather(hidden_up, "fs", axis=0, tiled=True))
    hidden = (jax.nn.silu(gate_total) * up_total).astype(jnp.bfloat16)
    hidden_part = jnp.dot(
        hidden,
        lax.all_gather(hidden_down, "fs", axis=1, tiled=True),
        preferred_element_type=jnp.float32,
    )
    hidden_own = lax.psum_scatter(
        hidden_part.astype(jnp.bfloat16), "tp", scatter_dimension=1, tiled=True
    ).astype(jnp.float32)
    hidden_energy = lax.psum(jnp.sum(hidden_own * hidden_own, axis=1), "tp")
    close_own = lax.dynamic_slice_in_dim(channel_post, feature_start, feature_width, 0)
    return (
        mid_own.astype(jnp.float32)
        + hidden_own * lax.rsqrt(hidden_energy / D + EPS)[:, None] * close_own
    ).astype(jnp.bfloat16)


def solution(mesh):
    in_specs = (
        P("fs", "tp"),
        P(),
        P("fs", "tp"),
        P("fs", "tp"),
        P(),
        P(),
        P(),
        P(),
        P(),
        P("tp", "fs"),
        P(),
        P(),
        P("fs", "tp"),
        P("fs", "tp"),
        P("tp", "fs"),
        P(),
    )
    out_specs = P("fs", "tp")
    return jax.shard_map(
        on_device, mesh=mesh, in_specs=in_specs, out_specs=out_specs, check_vma=False
    )
```

profile of v0, /device:TPU:0, one launch (start us, length us, event | category | flops | bytes accessed | tf_op | source)
XLA Modules:
  0.0 592.1 jit_solution(11456441102849634958)
XLA Ops:
  10.1 1.3 dynamic_slice.25
  12.3 21.9 %all-gather.8.cloned.1.call-done = bf16[512,2048]{1,0:T(8,128)(2,1)} async-done(((bf16[512,512]{1,0:T(8,128)(2,1)}), bf16[512,2048]{1,0:T(8,128)(2,1)}) %all-gather.8.cloned.1.call-update) | async-done | bytes 2097168 | tf_op jit(solution)/shard_map/all_gather | solution.py:85
  34.2 2.1 fusion.5
  36.3 40.3 %all-gather.10.cloned.1.call-done = bf16[2048,256]{1,0:T(8,128)(2,1)} async-done(((bf16[256,256]{1,0:T(8,128)(2,1)}), bf16[2048,256]{1,0:T(8,128)(2,1)}) %all-gather.10.cloned.1.call-update) | async-done | bytes 1048592 | tf_op jit(solution)/shard_map/all_gather | solution.py:92
  76.6 2.6 fusion.22
  80.7 2.1 fusion.21
  82.9 1.3 fusion.17
  85.2 2.0 copy.33
  89.2 2.5 multiply_exponential_fusion
  92.3 1.4 slice.487
  93.7 1.4 slice.485
  95.0 1.4 slice.489
  106.9 1.4 fusion.101
  108.4 1.4 slice.510
  109.7 1.4 slice.511
  111.1 1.4 slice.509
  112.4 1.4 slice.513
  113.8 1.4 fusion.103
  116.4 1.3 slice.515
  117.7 1.3 slice.519
  119.0 1.3 fusion.105
  124.2 1.3 slice.525
  133.3 1.3 fusion.107
  136.5 1.3 slice.537
  139.0 1.3 slice.514
  142.3 1.4 slice.541
  153.2 1.3 slice.561
  165.9 1.4 slice.554
  167.3 1.4 slice.624
  179.0 1.7 pad.132
  181.4 1.7 pad.131
  183.9 1.7 pad.150
  185.6 1.8 slice.555
  187.4 3.0 slice.625
  191.6 1.9 add.409
  193.5 3.4 rev.2
  197.0 5.7 convolution_convert_fusion
  205.1 47.9 %all-reduce.39.cloned.1.call-done = bf16[512,2048]{1,0:T(8,128)(2,1)} async-done(((bf16[512,2048]{1,0:T(8,128)(2,1)}), bf16[512,2048]{1,0:T(8,128)(2,1)}) %all-reduce.39.cloned.1.call-update) | async-done | bytes 2097168 | tf_op jit(solution)/shard_map/psum | solution.py:112
  253.0 2.1 fusion
  255.1 4.0 fusion.2
  259.2 88.3 %all-gather.16.cloned.1.call-done = bf16[2048,1408]{1,0:T(8,128)(2,1)} async-done(((bf16[256,1408]{1,0:T(8,128)(2,1)}), bf16[2048,1408]{1,0:T(8,128)(2,1)}) %all-gather.16.cloned.1.call-update) | async-done | bytes 5767184 | tf_op jit(solution)/shard_map/all_gather | solution.py:120
  347.5 8.5 %fusion.30 = f32[512,1408]{1,0:T(8,128)} fusion(bf16[2048,1408]{1,0:T(8,128)(2,1)} %all-gather.16.cloned.1.call-done, bf16[512,2048]{1,0:T(8,128)(2,1)} %get-tuple-element.6, f32[2048]{0:T(1024)S(1)} %copy-done.23, f32[512]{0:T(512)S(1)} %add_rsqrt_fusion.1), kind=kOutput, calls=%fused_computation.47 | convolution fusion | flops 2956984320 | bytes 10758144 | tf_op jit(solution)/shard_map/dot_general | solution.py:58
  356.0 84.2 %all-gather.18.cloned.1.call-done = bf16[2048,1408]{1,0:T(8,128)(2,1)} async-done(((bf16[256,1408]{1,0:T(8,128)(2,1)}), bf16[2048,1408]{1,0:T(8,128)(2,1)}) %all-gather.18.cloned.1.call-update) | async-done | bytes 5767184 | tf_op jit(solution)/shard_map/all_gather | solution.py:121
  440.2 93.4 %all-gather.20.cloned.1.call-done = bf16[1408,2048]{1,0:T(8,128)(2,1)} async-done(((bf16[1408,256]{1,0:T(8,128)(2,1)}), bf16[1408,2048]{1,0:T(8,128)(2,1)}) %all-gather.20.cloned.1.call-update) | async-done | bytes 5767184 | tf_op jit(solution)/shard_map/all_gather | solution.py:125
  533.6 13.4 %convolution_convert_fusion.1 = bf16[512,2048]{1,0:T(8,128)(2,1)} fusion(bf16[1408,2048]{1,0:T(8,128)(2,1)} %all-gather.20.cloned.1.call-done, bf16[2048,1408]{1,0:T(8,128)(2,1)} %all-gather.18.cloned.1.call-done, f32[512,1408]{1,0:T(8,128)} %fusion.30, bf16[512,2048]{1,0:T(8,128)(2,1)S(1)} %copy-done.2, f32[2048]{0:T(1024)S(1)} %copy-done.23, ...), kind=kOutput, calls=%fused_computation.19 | convolution fusion | flops 5915148288 | bytes 18622464 | tf_op jit(solution)/shard_map/dot_general | solution.py:123
  547.7 28.7 %reduce-scatter.2.cloned.1.call-done = bf16[512,512]{1,0:T(8,128)(2,1)} async-done(((bf16[512,2048]{1,0:T(8,128)(2,1)}), bf16[512,512]{1,0:T(8,128)(2,1)}) %reduce-scatter.2.cloned.1.call-update) | async-done | bytes 524304 | tf_op jit(solution)/shard_map/reduce_scatter | solution.py:128
  577.7 5.8 psum.15
  583.5 2.1 fusion.27
  (269 shorter events, 75.2 us)
Async XLA Ops:
  6.5 73.2 %copy-start = (bf16[2,16,64,64]{3,2,1,0:T(8,128)(2,1)S(1)}, bf16[2,16,64,64]{3,2,1,0:T(8,128)(2,1)}, u32[]{:S(2)}) copy-start(bf16[2,16,64,64]{3,2,1,0:T(8,128)(2,1)} %param.22) | copy-start | bytes 786436
  6.5 27.7 %all-gather.8.cloned.1.call-start = ((), (), s32[]{:S(2)}) async-start(), calls=%async_computation.1 | async-start | bytes 2621440 | tf_op jit(solution)/shard_map/all_gather | solution.py:85
  7.3 69.4 %all-gather.10.cloned.1.call-start = ((), (), s32[]{:S(2)}) async-start(), calls=%async_computation.2 | async-start | bytes 1179648 | tf_op jit(solution)/shard_map/all_gather | solution.py:92
  8.0 189.0 %all-gather.12.cloned.1.call-start = ((), (), s32[]{:S(2)}) async-start(), calls=%async_computation.3 | async-start | bytes 1179648 | tf_op jit(solution)/shard_map/all_gather | solution.py:93
  8.7 188.2 %all-gather.14.cloned.1.call-start = ((), (), s32[]{:S(2)}) async-start(), calls=%async_computation.4 | async-start | bytes 1179648 | tf_op jit(solution)/shard_map/all_gather | solution.py:109
  9.3 243.7 %all-reduce.39.cloned.1.call-start = ((), (), s32[]{:S(2)}) async-start(), calls=%async_computation.5 | async-start | bytes 4194304 | tf_op jit(solution)/shard_map/psum | solution.py:112
  36.3 43.0 %copy-start.19 = (f32[512]{0:T(512)}, f32[512]{0:T(512)S(1)}, u32[]{:S(2)}) copy-start(f32[512]{0:T(512)S(1)} %add_rsqrt_fusion.3) | copy-start | bytes 6148
  155.7 22.4 %copy-start.3 = (f32[127,256]{1,0:T(8,128)S(1)}, f32[127,256]{1,0:T(8,128)}, u32[]{:S(2)}) copy-start(f32[127,256]{1,0:T(8,128)} %slice.547) | copy-start | bytes 390148
  168.7 14.4 %copy-start.17 = (f32[1,256]{1,0:T(1,128)S(1)}, f32[1,256]{1,0:T(1,128)}, u32[]{:S(2)}) copy-start(f32[1,256]{1,0:T(1,128)} %get-tuple-element.41) | copy-start | bytes 3076
  168.7 14.4 %copy-start.18 = (f32[1,256]{1,0:T(1,128)S(1)}, f32[1,256]{1,0:T(1,128)}, u32[]{:S(2)}) copy-start(f32[1,256]{1,0:T(1,128)} %get-tuple-element.42) | copy-start | bytes 3076
  168.7 14.4 %copy-start.9 = (f32[2,256]{1,0:T(2,128)S(1)}, f32[2,256]{1,0:T(2,128)}, u32[]{:S(2)}) copy-start(f32[2,256]{1,0:T(2,128)} %pad_add_fusion) | copy-start | bytes 6148
  170.0 13.2 %copy-start.6 = (f32[3,256]{1,0:T(4,128)S(1)}, f32[3,256]{1,0:T(4,128)}, u32[]{:S(2)}) copy-start(f32[3,256]{1,0:T(4,128)} %slice.595) | copy-start | bytes 9220
  170.0 13.2 %copy-start.7 = (f32[3,256]{1,0:T(4,128)S(1)}, f32[3,256]{1,0:T(4,128)}, u32[]{:S(2)}) copy-start(f32[3,256]{1,0:T(4,128)} %slice.612) | copy-start | bytes 9220
  170.7 12.6 %copy-start.16 = (f32[1,256]{1,0:T(1,128)S(1)}, f32[1,256]{1,0:T(1,128)}, u32[]{:S(2)}) copy-start(f32[1,256]{1,0:T(1,128)} %slice.666) | copy-start | bytes 3076
  172.0 11.2 %copy-start.4 = (f32[7,256]{1,0:T(8,128)S(1)}, f32[7,256]{1,0:T(8,128)}, u32[]{:S(2)}) copy-start(f32[7,256]{1,0:T(8,128)} %slice.589) | copy-start | bytes 21508
  172.0 11.2 %copy-start.5 = (f32[7,256]{1,0:T(8,128)S(1)}, f32[7,256]{1,0:T(8,128)}, u32[]{:S(2)}) copy-start(f32[7,256]{1,0:T(8,128)} %slice.614) | copy-start | bytes 21508
  172.1 11.2 %copy-start.15 = (f32[1,256]{1,0:T(1,128)S(1)}, f32[1,256]{1,0:T(1,128)}, u32[]{:S(2)}) copy-start(f32[1,256]{1,0:T(1,128)} %slice.665) | copy-start | bytes 3076
  174.2 9.2 %copy-start.14 = (f32[1,256]{1,0:T(1,128)S(1)}, f32[1,256]{1,0:T(1,128)}, u32[]{:S(2)}) copy-start(f32[1,256]{1,0:T(1,128)} %slice.664) | copy-start | bytes 3076
  175.7 7.8 %copy-start.13 = (f32[1,256]{1,0:T(1,128)S(1)}, f32[1,256]{1,0:T(1,128)}, u32[]{:S(2)}) copy-start(f32[1,256]{1,0:T(1,128)} %slice.663) | copy-start | bytes 3076
  177.4 6.2 %copy-start.12 = (f32[1,256]{1,0:T(1,128)S(1)}, f32[1,256]{1,0:T(1,128)}, u32[]{:S(2)}) copy-start(f32[1,256]{1,0:T(1,128)} %slice.662) | copy-start | bytes 3076
  178.2 5.6 copy-start.11
  183.1 8.4 %copy-start.10 = (f32[1,256]{1,0:T(1,128)S(1)}, f32[1,256]{1,0:T(1,128)}, u32[]{:S(2)}) copy-start(f32[1,256]{1,0:T(1,128)} %slice.660) | copy-start | bytes 3076
  183.8 13.2 %copy-start.1 = (bf16[512,2048]{1,0:T(8,128)(2,1)S(1)}, bf16[512,2048]{1,0:T(8,128)(2,1)}, u32[]{:S(2)}) copy-start(bf16[512,2048]{1,0:T(8,128)(2,1)} %all-gather.8.cloned.1.call-done) | copy-start | bytes 6291460
  183.8 13.2 %copy-start.20 = (f32[512]{0:T(512)S(1)}, f32[512]{0:T(512)}, u32[]{:S(2)}) copy-start(f32[512]{0:T(512)} %copy-done.19) | copy-start | bytes 6148
  183.8 13.2 %copy-start.21 = (f32[256]{0:T(256)S(1)}, f32[256]{0:T(256)}, u32[]{:S(2)}) copy-start(f32[256]{0:T(256)} %dynamic_slice.25) | copy-start | bytes 3076
  183.8 13.2 %copy-start.22 = (f32[2048]{0:T(1024)S(1)}, f32[2048]{0:T(1024)}, u32[]{:S(2)}) copy-start(f32[2048]{0:T(1024)} %param.17) | copy-start | bytes 24580
  202.7 52.4 %copy-start.8 = (f32[2048]{0:T(1024)S(1)}, f32[2048]{0:T(1024)}, u32[]{:S(2)}) copy-start(f32[2048]{0:T(1024)} %param.26) | copy-start | bytes 24580
  202.8 144.7 %all-gather.16.cloned.1.call-start = ((), (), s32[]{:S(2)}) async-start(), calls=%async_computation.6 | async-start | bytes 6488064 | tf_op jit(solution)/shard_map/all_gather | solution.py:120
  203.3 236.9 %all-gather.18.cloned.1.call-start = ((), (), s32[]{:S(2)}) async-start(), calls=%async_computation.7 | async-start | bytes 6488064 | tf_op jit(solution)/shard_map/all_gather | solution.py:121
  204.1 329.5 %all-gather.20.cloned.1.call-start = ((), (), s32[]{:S(2)}) async-start(), calls=%async_computation.8 | async-start | bytes 6488064 | tf_op jit(solution)/shard_map/all_gather | solution.py:125
  204.8 142.7 %copy-start.23 = (f32[2048]{0:T(1024)S(1)}, f32[2048]{0:T(1024)}, u32[]{:S(2)}) copy-start(f32[2048]{0:T(1024)} %param.27) | copy-start | bytes 24580
  204.8 371.6 %reduce-scatter.2.cloned.1.call-start = ((), (), s32[]{:S(2)}) async-start(), calls=%async_computation.9 | async-start | bytes 2621440 | tf_op jit(solution)/shard_map/reduce_scatter | solution.py:128
  347.5 186.1 %copy-start.2 = (bf16[512,2048]{1,0:T(8,128)(2,1)S(1)}, bf16[512,2048]{1,0:T(8,128)(2,1)}, u32[]{:S(2)}) copy-start(bf16[512,2048]{1,0:T(8,128)(2,1)} %get-tuple-element.6) | copy-start | bytes 6291460
Sparse Core Ops, SparseCore 0:
  8.9 25.2 all-gather.7
  36.3 40.2 all-gather.9
  78.8 38.9 all-gather.11
  119.7 38.0 all-gather.13
  202.9 50.1 all-reduce.38
  255.1 92.3 all-gather.15
  349.7 90.4 all-gather.17
  442.2 91.2 all-gather.19
  547.1 29.3 reduce-scatter.1
where the time goes:
time: 595 us; the launch traced here: 592 us
  waiting for transfers between devices  409 us (69%)
  local copies, waits for them, and re-layouts  84 us (14%)
  other arithmetic  43.5 us (7%)
  matrix products  34.6 us (6%)
  between operations  14.2 us (2%)
    all_gather x1, waiting for transfers between devices, on_device(): lax.all_gather(hidden_down, 'fs', axis=1, tiled=True)  93.4 us
    all_gather x1, waiting for transfers between devices, on_device(): lax.all_gather(hidden_gate, 'fs', axis=0, tiled=True)  88.3 us
    all_gather x1, waiting for transfers between devices, on_device(): up_total = add_channel(lax.all_gather(hidden_up, 'fs', axis=0, tiled=True))  84.2 us
    slice x112, local copies, waits for them, and re-layouts, linear_scan(): lax.associative_scan(combine, (decay, inflow), axis=0, reverse=reverse)[1]  66.9 us
    psum x1, waiting for transfers between devices, on_device(): lax.psum(branch_part.astype(jnp.bfloat16), 'tp').astype(jnp.float32)  47.9 us
    all_gather x1, waiting for transfers between devices, on_device(): recur_total = add_mixer(lax.all_gather(recur_in, 'fs', axis=0, tiled=True))  40.3 us
    reduce_scatter x1, waiting for transfers between devices, on_device(): lax.psum_scatter(hidden_part.astype(jnp.bfloat16), 'tp', scatter_dimensio...  28.7 us
    all_gather x1, waiting for transfers between devices, on_device(): gathered_in = lax.all_gather(tokens, 'tp', axis=1, tiled=True)  21.9 us
  transfers between devices with their start and end apart: 9, of which 7 were waited for; matrix products, arithmetic and copies ran while one was open for 24% of the time, Pallas kernels for 0%

commit v1 on v0

--- a/solution.py
+++ b/solution.py
@@ -122,7 +122,7 @@
     hidden = (jax.nn.silu(gate_total) * up_total).astype(jnp.bfloat16)
     hidden_part = jnp.dot(
         hidden,
-        lax.all_gather(hidden_down, "fs", axis=1, tiled=True),
+        jnp.concatenate(lax.all_gather(hidden_down, "fs"), axis=1),
         preferred_element_type=jnp.float32,
     )
     hidden_own = lax.psum_scatter(

time: 595 us -> 554 us (0.931)
  local copies, waits for them, and re-layouts: 84 us -> 47.9 us
  other arithmetic: 43.5 us -> 26.8 us
  waiting for transfers between devices: 409 us -> 424 us
    slice x112, local copies, waits for them, and re-layouts: 66.9 us -> 24.9 us  [linear_scan(): lax.associative_scan(combine, (decay, inflow), axis=0, reverse=reverse)[1]]
    all_gather x1, waiting for transfers between devices: 0.02 us -> 21.9 us  [on_device(): lax.all_gather(recur_out, 'fs', axis=1, tiled=True)]
    mul x14, other arithmetic: 10.6 us -> 1.28 us  [combine(): return (former[0] * latter[0], latter[0] * former[1] + latter[1])]
    reshape x0 -> x1, local copies, waits for them, and re-layouts: none -> 8.33 us  [on_device(): jnp.concatenate(lax.all_gather(hidden_down, 'fs'), axis=1)]
  transfers between devices with their start and end apart: 9 -> 9, of which waited for: 7 -> 8; matrix products, arithmetic and copies ran while one was open for 24% -> 16% of each run, Pallas kernels for 0% -> 0%
where the time goes in v1:
time: 554 us; the launch traced here: 552 us
  waiting for transfers between devices  424 us (77%)
  local copies, waits for them, and re-layouts  47.9 us (9%)
  matrix products  33.7 us (6%)
  other arithmetic  26.8 us (5%)
  between operations  14.3 us (3%)
  blocking collectives  5.76 us (1%)
    all_gather x1, waiting for transfers between devices, on_device(): lax.all_gather(hidden_down, 'fs')  88.3 us
    all_gather x1, waiting for transfers between devices, on_device(): up_total = add_channel(lax.all_gather(hidden_up, 'fs', axis=0, tiled=True))  85 us
    all_gather x1, waiting for transfers between devices, on_device(): lax.all_gather(hidden_gate, 'fs', axis=0, tiled=True)  84.4 us
    psum x1, waiting for transfers between devices, on_device(): lax.psum(branch_part.astype(jnp.bfloat16), 'tp').astype(jnp.float32)  48.4 us
    all_gather x1, waiting for transfers between devices, on_device(): recur_total = add_mixer(lax.all_gather(recur_in, 'fs', axis=0, tiled=True))  40.3 us
    reduce_scatter x1, waiting for transfers between devices, on_device(): lax.psum_scatter(hidden_part.astype(jnp.bfloat16), 'tp', scatter_dimensio...  28.7 us
    slice x112, local copies, waits for them, and re-layouts, linear_scan(): lax.associative_scan(combine, (decay, inflow), axis=0, reverse=reverse)[1]  24.9 us
    all_gather x1, waiting for transfers between devices, on_device(): gathered_in = lax.all_gather(tokens, 'tp', axis=1, tiled=True)  22 us
  transfers between devices with their start and end apart: 9, of which 8 were waited for; matrix products, arithmetic and copies ran while one was open for 16% of the time, Pallas kernels for 0%

profile of v1, /device:TPU:0, one launch (start us, length us, event | category | flops | bytes accessed | tf_op | source)
XLA Modules:
  0.0 552.4 jit_solution(5989394387770745416)
XLA Ops:
  6.5 0.7 all-gather.9.cloned.1.call-update
  7.3 0.7 all-gather.11.cloned.1.call-update
  10.1 1.3 dynamic_slice.25
  11.4 0.8 fusion.85
  12.2 22.0 %all-gather.9.cloned.1.call-done = bf16[512,2048]{1,0:T(8,128)(2,1)} async-done(((bf16[512,512]{1,0:T(8,128)(2,1)}), bf16[512,2048]{1,0:T(8,128)(2,1)}) %all-gather.9.cloned.1.call-update) | async-done | bytes 2097168 | tf_op jit(solution)/shard_map/all_gather | solution.py:85
  34.2 2.1 fusion.5
  36.3 40.3 %all-gather.11.cloned.1.call-done = bf16[2048,256]{1,0:T(8,128)(2,1)} async-done(((bf16[256,256]{1,0:T(8,128)(2,1)}), bf16[2048,256]{1,0:T(8,128)(2,1)}) %all-gather.11.cloned.1.call-update) | async-done | bytes 1048592 | tf_op jit(solution)/shard_map/all_gather | solution.py:92
  76.6 2.6 fusion.22
  80.8 2.1 fusion.21
  82.9 1.3 fusion.17
  84.4 2.1 copy.40
  86.5 1.0 copy.36
  87.5 1.0 copy.38
  88.5 2.3 multiply_exponential_fusion
  92.1 1.4 slice.489
  93.5 1.0 fusion.95
  110.3 1.4 slice.554
  111.7 1.4 slice.624
  114.4 0.7 pad.118
  115.1 0.7 fusion.75
  116.5 0.7 fusion.73
  117.9 0.7 fusion.71
  119.3 0.8 fusion.69
  121.2 1.7 pad.132
  122.9 1.7 pad.131
  125.5 2.0 slice.555
  127.5 3.0 slice.625
  130.5 1.0 fusion.57
  131.7 0.9 add.409
  132.5 3.4 rev.2
  136.0 21.9 %all-gather.15.cloned.1.call-done = bf16[256,2048]{1,0:T(8,128)(2,1)} async-done(((bf16[256,256]{1,0:T(8,128)(2,1)}), bf16[256,2048]{1,0:T(8,128)(2,1)}) %all-gather.15.cloned.1.call-update) | async-done | bytes 1048592 | tf_op jit(solution)/shard_map/all_gather | solution.py:109
  157.9 5.6 %convolution_convert_fusion = bf16[512,2048]{1,0:T(8,128)(2,1)} fusion(bf16[256,2048]{1,0:T(8,128)(2,1)} %all-gather.15.cloned.1.call-done, bf16[2048,256]{1,0:T(8,128)(2,1)} %all-gather.13.cloned.1.call-done, bf16[512,2048]{1,0:T(8,128)(2,1)S(1)} %copy-done.2, f32[2048]{0:T(1024)S(1)} %copy-done.12, f32[512]{0:T(512)S(1)} %copy-done.10, ...), kind=kOutput, calls=%fused_computation.17 | convolution fusion | flops 1080950784 | bytes 7875584 | tf_op jit(solution)/shard_map/dot_general | solution.py:107
  164.1 0.7 all-gather.17.cloned.1.call-update
  164.9 0.7 all-gather.19.cloned.1.call-update
  165.6 48.4 %all-reduce.39.cloned.1.call-done = bf16[512,2048]{1,0:T(8,128)(2,1)} async-done(((bf16[512,2048]{1,0:T(8,128)(2,1)}), bf16[512,2048]{1,0:T(8,128)(2,1)}) %all-reduce.39.cloned.1.call-update) | async-done | bytes 2097168 | tf_op jit(solution)/shard_map/psum | solution.py:112
  214.1 2.1 fusion
  216.2 4.1 fusion.2
  220.3 88.3 %all-gather.21.cloned.1.call-done = bf16[11264,256]{1,0:T(8,128)(2,1)} async-done(((bf16[1408,256]{1,0:T(8,128)(2,1)}), bf16[11264,256]{1,0:T(8,128)(2,1)}) %all-gather.21.cloned.1.call-update) | async-done | bytes 5767184 | tf_op jit(solution)/shard_map/all_gather | solution.py:125
  308.5 8.3 %copy.41 = bf16[1408,8,256]{0,2,1:T(8,128)(2,1)} copy(bf16[1408,8,256]{2,0,1:T(8,128)(2,1)} %bitcast.49) | data formatting | bytes 11534336 | tf_op jit(solution)/shard_map/reshape | solution.py:125
  316.9 84.4 %all-gather.17.cloned.1.call-done = bf16[2048,1408]{1,0:T(8,128)(2,1)} async-done(((bf16[256,1408]{1,0:T(8,128)(2,1)}), bf16[2048,1408]{1,0:T(8,128)(2,1)}) %all-gather.17.cloned.1.call-update) | async-done | bytes 5767184 | tf_op jit(solution)/shard_map/all_gather | solution.py:120
  401.2 7.7 %fusion.30 = f32[512,1408]{1,0:T(8,128)} fusion(bf16[2048,1408]{1,0:T(8,128)(2,1)} %all-gather.17.cloned.1.call-done, bf16[512,2048]{1,0:T(8,128)(2,1)S(1)} %copy-done.3, f32[2048]{0:T(1024)S(1)} %copy-done.13, f32[512]{0:T(512)S(1)} %add_rsqrt_fusion.1), kind=kOutput, calls=%fused_computation.47 | convolution fusion | flops 2956984320 | bytes 10758144 | tf_op jit(solution)/shard_map/dot_general | solution.py:58
  408.9 85.0 %all-gather.19.cloned.1.call-done = bf16[2048,1408]{1,0:T(8,128)(2,1)} async-done(((bf16[256,1408]{1,0:T(8,128)(2,1)}), bf16[2048,1408]{1,0:T(8,128)(2,1)}) %all-gather.19.cloned.1.call-update) | async-done | bytes 5767184 | tf_op jit(solution)/shard_map/all_gather | solution.py:121
  493.9 13.3 %convolution_convert_fusion.1 = bf16[512,2048]{1,0:T(8,128)(2,1)} fusion(bf16[1408,2048]{0,1:T(8,128)(2,1)} %bitcast.50, bf16[2048,1408]{1,0:T(8,128)(2,1)} %all-gather.19.cloned.1.call-done, f32[512,1408]{1,0:T(8,128)} %fusion.30, bf16[512,2048]{1,0:T(8,128)(2,1)S(1)} %copy-done.3, f32[2048]{0:T(1024)S(1)} %copy-done.13, f32[512]{0:T(512)S(1)} %add_rsqrt_fusion.1), kind=kOutput, calls=%fused_computation.19 | convolution fusion | flops 5915148288 | bytes 18622464 | tf_op jit(solution)/shard_map/dot_general | solution.py:123
  507.3 0.8 dynamic_slice.27
  508.0 28.7 %reduce-scatter.2.cloned.1.call-done = bf16[512,512]{1,0:T(8,128)(2,1)} async-done(((bf16[512,2048]{1,0:T(8,128)(2,1)}), bf16[512,512]{1,0:T(8,128)(2,1)}) %reduce-scatter.2.cloned.1.call-update) | async-done | bytes 524304 | tf_op jit(solution)/shard_map/reduce_scatter | solution.py:128
  536.8 1.2 fusion.24
  538.0 5.8 %psum.15 = f32[512]{0:T(512)S(1)} all-reduce(f32[512]{0:T(512)S(1)} %fusion.24), channel_id=1, replica_groups=mesh['fs'=8,'tp'=4] {'tp'}, use_global_device_ids=true, to_apply=%region_6.7 | all-reduce | flops 512 | bytes 4096 | tf_op jit(solution)/shard_map/psum | solution.py:131
  543.7 2.1 fusion.27
  (250 shorter events, 26.1 us)
Async XLA Ops:
  6.5 73.2 %copy-start = (bf16[2,16,64,64]{3,2,1,0:T(8,128)(2,1)S(1)}, bf16[2,16,64,64]{3,2,1,0:T(8,128)(2,1)}, u32[]{:S(2)}) copy-start(bf16[2,16,64,64]{3,2,1,0:T(8,128)(2,1)} %param.22) | copy-start | bytes 786436
  6.5 27.7 %all-gather.9.cloned.1.call-start = ((), (), s32[]{:S(2)}) async-start(), calls=%async_computation.1 | async-start | bytes 2621440 | tf_op jit(solution)/shard_map/all_gather | solution.py:85
  7.3 69.4 %all-gather.11.cloned.1.call-start = ((), (), s32[]{:S(2)}) async-start(), calls=%async_computation.2 | async-start | bytes 1179648 | tf_op jit(solution)/shard_map/all_gather | solution.py:92
  8.0 128.0 %all-gather.13.cloned.1.call-start = ((), (), s32[]{:S(2)}) async-start(), calls=%async_computation.3 | async-start | bytes 1179648 | tf_op jit(solution)/shard_map/all_gather | solution.py:93
  8.7 149.1 %all-gather.15.cloned.1.call-start = ((), (), s32[]{:S(2)}) async-start(), calls=%async_computation.4 | async-start | bytes 1179648 | tf_op jit(solution)/shard_map/all_gather | solution.py:109
  9.3 204.7 %all-reduce.39.cloned.1.call-start = ((), (), s32[]{:S(2)}) async-start(), calls=%async_computation.5 | async-start | bytes 4194304 | tf_op jit(solution)/shard_map/psum | solution.py:112
  36.3 43.9 %copy-start.9 = (f32[512]{0:T(512)}, f32[512]{0:T(512)S(1)}, u32[]{:S(2)}) copy-start(f32[512]{0:T(512)S(1)} %add_rsqrt_fusion.3) | copy-start | bytes 6148
  108.4 12.5 %copy-start.7 = (f32[1,256]{1,0:T(1,128)S(1)}, f32[1,256]{1,0:T(1,128)}, u32[]{:S(2)}) copy-start(f32[1,256]{1,0:T(1,128)} %slice.632) | copy-start | bytes 3076
  108.6 12.4 %copy-start.6 = (f32[1,256]{1,0:T(1,128)S(1)}, f32[1,256]{1,0:T(1,128)}, u32[]{:S(2)}) copy-start(f32[1,256]{1,0:T(1,128)} %slice.631) | copy-start | bytes 3076
  110.1 12.8 %copy-start.5 = (f32[1,256]{1,0:T(1,128)S(1)}, f32[1,256]{1,0:T(1,128)}, u32[]{:S(2)}) copy-start(f32[1,256]{1,0:T(1,128)} %slice.630) | copy-start | bytes 3076
  124.7 6.9 %copy-start.8 = (f32[1,256]{1,0:T(1,128)S(1)}, f32[1,256]{1,0:T(1,128)}, u32[]{:S(2)}) copy-start(f32[1,256]{1,0:T(1,128)} %slice.660) | copy-start | bytes 3076
  125.3 32.6 %copy-start.2 = (bf16[512,2048]{1,0:T(8,128)(2,1)S(1)}, bf16[512,2048]{1,0:T(8,128)(2,1)}, u32[]{:S(2)}) copy-start(bf16[512,2048]{1,0:T(8,128)(2,1)} %all-gather.9.cloned.1.call-done) | copy-start | bytes 6291460
  125.3 32.6 %copy-start.10 = (f32[512]{0:T(512)S(1)}, f32[512]{0:T(512)}, u32[]{:S(2)}) copy-start(f32[512]{0:T(512)} %copy-done.9) | copy-start | bytes 6148
  125.3 32.6 %copy-start.11 = (f32[256]{0:T(256)S(1)}, f32[256]{0:T(256)}, u32[]{:S(2)}) copy-start(f32[256]{0:T(256)} %dynamic_slice.25) | copy-start | bytes 3076
  125.3 32.5 %copy-start.12 = (f32[2048]{0:T(1024)S(1)}, f32[2048]{0:T(1024)}, u32[]{:S(2)}) copy-start(f32[2048]{0:T(1024)} %param.17) | copy-start | bytes 24580
  163.5 52.7 %copy-start.4 = (f32[2048]{0:T(1024)S(1)}, f32[2048]{0:T(1024)}, u32[]{:S(2)}) copy-start(f32[2048]{0:T(1024)} %param.26) | copy-start | bytes 24580
  163.5 145.0 %all-gather.21.cloned.1.call-start = ((), (), s32[]{:S(2)}) async-start(), calls=%async_computation.9 | async-start | bytes 6488064 | tf_op jit(solution)/shard_map/all_gather | solution.py:125
  164.1 237.1 %all-gather.17.cloned.1.call-start = ((), (), s32[]{:S(2)}) async-start(), calls=%async_computation.6 | async-start | bytes 6488064 | tf_op jit(solution)/shard_map/all_gather | solution.py:120
  164.8 329.1 %all-gather.19.cloned.1.call-start = ((), (), s32[]{:S(2)}) async-start(), calls=%async_computation.7 | async-start | bytes 6488064 | tf_op jit(solution)/shard_map/all_gather | solution.py:121
  165.6 371.2 %reduce-scatter.2.cloned.1.call-start = ((), (), s32[]{:S(2)}) async-start(), calls=%async_computation.8 | async-start | bytes 2621440 | tf_op jit(solution)/shard_map/reduce_scatter | solution.py:128
  308.5 92.7 %copy-start.3 = (bf16[512,2048]{1,0:T(8,128)(2,1)S(1)}, bf16[512,2048]{1,0:T(8,128)(2,1)}, u32[]{:S(2)}) copy-start(bf16[512,2048]{1,0:T(8,128)(2,1)} %get-tuple-element.6) | copy-start | bytes 6291460
  308.5 92.7 %copy-start.13 = (f32[2048]{0:T(1024)S(1)}, f32[2048]{0:T(1024)}, u32[]{:S(2)}) copy-start(f32[2048]{0:T(1024)} %param.27) | copy-start | bytes 24580
  493.9 51.9 %copy-start.1 = (bf16[2,16,64,64]{3,2,1,0:T(8,128)(2,1)S(1)}, bf16[2,16,64,64]{3,2,1,0:T(8,128)(2,1)}, u32[]{:S(2)}) copy-start(bf16[2,16,64,64]{3,2,1,0:T(8,128)(2,1)} %param.22) | copy-start | bytes 786436
Sparse Core Ops, SparseCore 0:
  8.9 25.2 all-gather.8
  36.3 40.2 all-gather.10
  78.8 38.9 all-gather.12
  119.7 38.0 all-gather.14
  163.6 50.3 all-reduce.38
  216.1 92.3 all-gather.20
  310.7 90.4 all-gather.16
  403.4 90.4 all-gather.18
  507.4 29.3 reduce-scatter.1
